TPU v7x, 32 devices: a whole 2x2x4 slice. The times are simulated.
32 devices in a mesh: sp: 4 (over y, core), dp: 8 (over z, x).
Axes of the slice: x: 2, y: 2, z: 4, core: 2. Of those that a mesh axis runs over, the one named last changes fastest.
Arguments:
- stream: bfloat16 [8, 512, 2064], P('dp', 'sp'), may hold values from -6 to 6
- mix_gain: float32 [2064], replicated, may hold values from 0.1 to 1.9
- query_weight: bfloat16 [2064, 2048], P('dp'), may hold values from -0.125 to 0.125
- query_gain: float32 [128], replicated, may hold values from 0.1 to 1.9
- keys: bfloat16 [8, 512, 512], P('dp', 'sp'), may hold values from -6 to 6
- key_gain: float32 [128], replicated, may hold values from 0.1 to 1.9
- values: bfloat16 [8, 512, 512], P('dp', 'sp'), may hold values from -48 to 48
- stick_offset: float32 [16], replicated, may hold values from -8.5 to -7, as said below
Outputs:
- attended: bfloat16 [8, 512, 2048], P('dp', 'sp')
Inputs may be any that keep to these rules, and one draw needn't show every extreme that they name: `stick_offset`: one offset for each query head, added to all of that head's scores.
All inputs are finite; a program needn't handle non-finite values.
Results may differ from a plain program's by a relative error of at most 0.012.
Values may be sent and summed in bfloat16 or wider, within the bound.
A program may use at most 64 MiB of HBM per device.

v0:
```python
import math
import jax
import jax.numpy as jnp
from jax import lax
from jax.sharding import PartitionSpec as P

norm_eps = 1e-06
row_block = 256
key_block = 128


def rms_scaled(inputs, gain):
    wide = inputs.astype(jnp.float32)
    scaled = wide * lax.rsqrt(jnp.mean(wide * wide, axis=-1, keepdims=True) + norm_eps) * gain
    return scaled.astype(jnp.bfloat16)


def stick_weights(scores, first_row):
    heads_here = scores.shape[0]
    rows_here = scores.shape[1]
    keys_here = scores.shape[2]
    width = math.gcd(keys_here, key_block)
    blocks_here = keys_here // width
    query_pos = first_row + jnp.arange(rows_here, dtype=jnp.int32)
    key_pos = jnp.arange(keys_here, dtype=jnp.int32)
    causal = key_pos[None, :] < query_pos[:, None]
    log_keep = jnp.where(causal, jax.nn.log_sigmoid(-scores), 0.0)
    pieces = log_keep.reshape(heads_here, rows_here, blocks_here, width)
    inner = jnp.arange(width, dtype=jnp.int32)
    upper = (inner[:, None] > inner[None, :]).astype(jnp.float32)
    local = jnp.einsum("hqbk,kj->hqbj", pieces, upper, precision=lax.Precision.HIGHEST)
    totals = jnp.sum(pieces, axis=3)
    later = lax.cumsum(totals, axis=2, reverse=True) - totals
    tail = (local + later[:, :, :, None]).reshape(heads_here, rows_here, keys_here)
    return jnp.where(causal, jnp.exp(jax.nn.log_sigmoid(scores) + tail), 0.0)


def body(stream, mix_gain, query_weight, query_gain, keys, key_gain, values, stick_offset):
    sp_count = lax.axis_size("sp")
    sp_index = lax.axis_index("sp")
    stream_rows = stream[0]
    tokens_dev = stream_rows.shape[0]
    head_width = query_gain.shape[0]
    heads_all = stick_offset.shape[0]
    heads_dev = heads_all // sp_count
    kv_count = keys.shape[2] // head_width
    group_size = sp_count // kv_count
    seq_length = tokens_dev * sp_count
    stacked = jnp.stack((keys[0], values[0]), axis=1).reshape(tokens_dev, 2, kv_count, head_width)
    copied = jnp.repeat(stacked, group_size, axis=2)
    arrived = lax.all_to_all(copied, "sp", split_axis=2, concat_axis=0, tiled=True)
    key_value = arrived[:, :, 0, :]
    normed = rms_scaled(stream_rows, mix_gain)
    columns = lax.dynamic_slice_in_dim(
        query_weight, sp_index * (heads_dev * head_width), heads_dev * head_width, 1
    )
    gathered = lax.all_gather(columns, "dp", axis=0, tiled=True)
    queries = jnp.dot(
        lax.all_gather(normed, "sp", axis=0, tiled=True),
        gathered,
        preferred_element_type=jnp.float32,
    ).astype(jnp.bfloat16)
    queries = lax.optimization_barrier(queries)
    mine = rms_scaled(queries.reshape(seq_length, heads_dev, head_width), query_gain)
    key_heads = rms_scaled(key_value[:, 0], key_gain)
    value_rows = key_value[:, 1]
    offsets = lax.dynamic_slice_in_dim(stick_offset, sp_index * heads_dev, heads_dev)
    block = math.gcd(seq_length, row_block)
    outputs = []
    for block_id in range(seq_length // block):
        first = block_id * block
        finish = first + block
        scores = jnp.einsum(
            "qhd,kd->hqk",
            mine[first:finish],
            key_heads[:finish],
            preferred_element_type=jnp.float32,
        )
        scores = scores * head_width ** (-0.5) + offsets[:, None, None]
        weights = stick_weights(scores, first).astype(jnp.bfloat16)
        outputs.append(
            jnp.einsum(
                "hqk,kd->qhd", weights, value_rows[:finish], preferred_element_type=jnp.float32
            )
        )
    attended = (
        jnp.concatenate(outputs, axis=0)
        .reshape(seq_length, heads_dev * head_width)
        .astype(jnp.bfloat16)
    )
    returned = lax.all_to_all(attended, "sp", split_axis=0, concat_axis=1, tiled=True)
    return returned[None]


def solution(mesh):
    return jax.shard_map(
        body,
        mesh=mesh,
        in_specs=(
            P("dp", "sp", None),
            P(),
            P("dp", None),
            P(),
            P("dp", "sp", None),
            P(),
            P("dp", "sp", None),
            P(),
        ),
        out_specs=P("dp", "sp", None),
        check_vma=False,
    )
```

profile of v0, /device:TPU:0, one launch (start us, length us, event | category | flops | bytes accessed | tf_op | source)
XLA Modules:
  0.0 124.1 jit_solution(3568556610034957392)
XLA Ops:
  6.6 1.2 copy-done
  7.8 0.7 dynamic-slice_bitcast_fusion
  8.6 1.3 %fusion.15 = f32[128]{0:T(128)S(1)} fusion(bf16[1,128,2064]{1,2,0:T(8,128)(2,1)} %param.8), kind=kLoop, calls=%fused_computation.31 | loop fusion | flops 792448 | bytes 528896 | tf_op jit(solution)/shard_map/reduce_sum | solution.py:14
  9.9 2.2 %fusion.17 = bf16[128,2064]{0,1:T(8,128)(2,1)} fusion(bf16[1,128,2064]{1,2,0:T(8,128)(2,1)} %param.8, f32[2064]{0:T(1024)} %param.9, f32[128]{0:T(128)S(1)} %add_rsqrt_fusion.2), kind=kLoop, calls=%fused_computation.33 | loop fusion | flops 1056768 | bytes 1065536 | tf_op jit(solution)/shard_map/convert_element_type | solution.py:15
  12.5 0.9 copy.56
  13.3 4.3 %all-to-all-start = ((bf16[128,2,4,128]{3,0,1,2:T(8,128)(2,1)}), bf16[128,2,4,128]{3,0,1,2:T(8,128)(2,1)S(1)}, u32[]{:S(2)}, u32[]{:S(2)}) async-start(bf16[128,2,4,128]{3,0,1,2:T(8,128)(2,1)} %copy.56), calls=%async_computation | async-start | bytes 524288 | tf_op jit(solution)/shard_map/all_to_all | solution.py:51
  17.7 0.7 iota_compare_fusion
  18.5 5.2 %all-to-all-done = bf16[128,2,4,128]{3,0,1,2:T(8,128)(2,1)S(1)} async-done(((bf16[128,2,4,128]{3,0,1,2:T(8,128)(2,1)}), bf16[128,2,4,128]{3,0,1,2:T(8,128)(2,1)S(1)}, u32[]{:S(2)}, u32[]{:S(2)}) %all-to-all-start) | async-done | bytes 262176 | tf_op jit(solution)/shard_map/all_to_all | solution.py:51
  23.8 0.8 fusion.29
  24.6 37.5 %all-gather.6.cloned.1.call-done = bf16[8,258,512]{2,1,0:T(8,128)(2,1)} async-done(((bf16[1,258,512]{2,1,0:T(8,128)(2,1)}), bf16[8,258,512]{2,1,0:T(8,128)(2,1)}) %all-gather.6.cloned.1.call-update) | async-done | bytes 2113552 | tf_op jit(solution)/shard_map/all_gather | solution.py:57
  62.1 1.9 %reshape.90 = bf16[2064,512]{1,0:T(8,128)(2,1)S(1)} reshape(bf16[8,258,512]{2,1,0:T(8,128)(2,1)} %all-gather.6.cloned.1.call-done) | data formatting | bytes 4227072
  63.9 21.1 %all-gather.4.cloned.1.call-done = bf16[512,2064]{0,1:T(8,128)(2,1)} async-done(((bf16[128,2064]{0,1:T(8,128)(2,1)}), bf16[512,2064]{0,1:T(8,128)(2,1)}) %all-gather.4.cloned.1.call-update) | async-done | bytes 2113552 | tf_op jit(solution)/shard_map/all_gather | solution.py:59
  85.1 3.8 %convolution_convert_fusion = bf16[512,512]{1,0:T(8,128)(2,1)} fusion(bf16[512,2064]{0,1:T(8,128)(2,1)} %all-gather.4.cloned.1.call-done, bf16[2064,512]{1,0:T(8,128)(2,1)S(1)} %reshape.90), kind=kOutput, calls=%fused_computation.26 | convolution fusion | flops 1082392576 | bytes 4751360 | tf_op jit(solution)/shard_map/dot_general | solution.py:58
  88.9 1.4 %reshape.88 = f32[512,4,128]{2,1,0:T(4,128)S(1)} reshape(bf16[512,512]{1,0:T(8,128)(2,1)} %convolution_convert_fusion) | data formatting | bytes 1572864 | tf_op jit(solution)/shard_map/convert_element_type | solution.py:13
  91.4 0.8 copy-done.5
  92.2 1.8 %bitcast_reduce_fusion.1 = (f32[4,256,2]{1,2,0:T(2,128)S(1)}, f32[4,256,256]{1,2,0:T(8,128)S(1)}, f32[4,256,256]{1,2,0:T(8,128)S(1)}) fusion(pred[256,256]{0,1:T(8,128)(4,1)S(1)} %iota_compare_fusion.1, f32[4]{0:T(128)S(1)} %dynamic_slice.7, bf16[512,4,128]{2,0,1:T(8,128)(2,1)S(1)} %fusion.26, bf16[512,128]{1,0:T(8,128)(2,1)} %fusion.29), kind=kOutput, calls=%fused_computation.71 | convolution fusion | flops 69990400 | bytes 2499072 | tf_op jit(solution)/shard_map/qhd,kd->hqk/dot_general | solution.py:73
  94.1 0.7 convolution_add_fusion.1
  94.8 0.8 fusion.22
  95.6 1.0 fusion.13
  96.6 3.1 %bitcast_reduce_fusion = (f32[4,256,4]{1,2,0:T(4,128)S(1)}, f32[4,256,512]{1,2,0:T(8,128)}, f32[512,256,4]{1,0,2:T(8,128)S(1)}) fusion(f32[4]{0:T(128)S(1)} %dynamic_slice.7, pred[256,512]{0,1:T(8,128)(4,1)S(1)} %copy-done.3, bf16[512,4,128]{2,0,1:T(8,128)(2,1)S(1)} %copy-done.6, bf16[512,128]{1,0:T(8,128)(2,1)S(1)} %copy-done.9), kind=kOutput, calls=%fused_computation.70 | convolution fusion | flops 139980800 | bytes 4735488 | tf_op jit(solution)/shard_map/qhd,kd->hqk/dot_general | solution.py:73
  99.7 2.9 %convolution_add_fusion = f32[4,256,4,128]{1,3,2,0:T(8,128)S(1)} fusion(f32[4,256,4,128]{1,3,2,0:T(8,128)} %bitcast.99, f32[4,256,4]{1,2,0:T(4,128)S(1)} %sub.15), kind=kOutput, calls=%fused_computation.19 | convolution fusion | flops 805847040 | bytes 4210688 | tf_op jit(solution)/shard_map/hqbk,kj->hqbj/dot_general | solution.py:31
  102.6 1.8 %fusion.4 = bf16[4,256,512]{1,2,0:T(8,128)(2,1)S(1)} fusion(f32[4,256,4,128]{1,3,2,0:T(8,128)S(1)} %convolution_add_fusion, f32[512,256,4]{1,0,2:T(8,128)S(1)} %get-tuple-element.9, f32[4]{0:T(128)S(1)} %dynamic_slice.7, pred[256,512]{0,1:T(8,128)(4,1)S(1)} %copy-done.4), kind=kLoop, calls=%fused_computation.8 | loop fusion | flops 6815744 | bytes 5373968 | tf_op jit(solution)/shard_map/convert_element_type | solution.py:80
  105.0 11.2 %all_to_all.28 = bf16[4,128,512]{1,2,0:T(8,128)(2,1)S(1)} all-to-all(bf16[4,128,512]{1,2,0:T(8,128)(2,1)S(1)} %copy.66), channel_id=1, replica_groups=mesh['sp'=4,'dp'=8] {'sp'}, dimensions={0} | all-to-all | bytes 1048576 | tf_op jit(solution)/shard_map/all_to_all | solution.py:91
  116.2 1.0 copy.67
  (50 shorter events, 2.4 us)
Async XLA Ops:
  6.5 1.2 copy-start
  6.5 5.6 %copy-start.7 = (bf16[1,128,512]{2,1,0:T(8,128)(2,1)S(1)}, bf16[1,128,512]{2,1,0:T(8,128)(2,1)}, u32[]{:S(2)}) copy-start(bf16[1,128,512]{2,1,0:T(8,128)(2,1)} %param.12) | copy-start | bytes 393220
  6.5 5.8 %copy-start.8 = (bf16[1,128,512]{2,1,0:T(8,128)(2,1)S(1)}, bf16[1,128,512]{2,1,0:T(8,128)(2,1)}, u32[]{:S(2)}) copy-start(bf16[1,128,512]{2,1,0:T(8,128)(2,1)} %param.14) | copy-start | bytes 393220
  6.5 55.5 %all-gather.6.cloned.1.call-start = ((), (), s32[]{:S(2)}) async-start(), calls=%async_computation.3 | async-start | bytes 2433024 | tf_op jit(solution)/shard_map/all_gather | solution.py:57
  8.5 9.1 %copy-start.12 = (f32[16]{0:T(128)S(1)}, f32[16]{0:T(128)}, u32[]{:S(2)}) copy-start(f32[16]{0:T(128)} %param.15) | copy-start | bytes 196
  8.5 76.5 %all-gather.4.cloned.1.call-start = ((), (), s32[]{:S(2)}) async-start(), calls=%async_computation.2 | async-start | bytes 2641920 | tf_op jit(solution)/shard_map/all_gather | solution.py:59
  9.9 13.9 %copy-start.10 = (f32[128]{0:T(128)S(1)}, f32[128]{0:T(128)}, u32[]{:S(2)}) copy-start(f32[128]{0:T(128)} %param.13) | copy-start | bytes 1540
  13.3 10.3 %all-to-all-start = ((bf16[128,2,4,128]{3,0,1,2:T(8,128)(2,1)}), bf16[128,2,4,128]{3,0,1,2:T(8,128)(2,1)S(1)}, u32[]{:S(2)}, u32[]{:S(2)}) async-start(bf16[128,2,4,128]{3,0,1,2:T(8,128)(2,1)} %copy.56), calls=%async_computation | async-start | bytes 524288 | tf_op jit(solution)/shard_map/all_to_all | solution.py:51
  88.9 2.2 %copy-start.1 = (bf16[512,512]{1,0:T(8,128)(2,1)S(1)}, bf16[512,512]{1,0:T(8,128)(2,1)}, u32[]{:S(2)}) copy-start(bf16[512,512]{1,0:T(8,128)(2,1)} %convolution_convert_fusion) | copy-start | bytes 1572868
  88.9 2.2 %copy-start.11 = (f32[128]{0:T(128)S(1)}, f32[128]{0:T(128)}, u32[]{:S(2)}) copy-start(f32[128]{0:T(128)} %param.11) | copy-start | bytes 1540
  91.4 0.8 copy-start.5
  94.7 1.8 %copy-start.3 = (pred[256,512]{0,1:T(8,128)(4,1)S(1)}, pred[256,512]{0,1:T(8,128)(4,1)}, u32[]{:S(2)}) copy-start(pred[256,512]{0,1:T(8,128)(4,1)} %iota_compare_fusion) | copy-start | bytes 393220
  94.7 1.8 %copy-start.6 = (bf16[512,4,128]{2,0,1:T(8,128)(2,1)S(1)}, bf16[512,4,128]{2,0,1:T(8,128)(2,1)}, u32[]{:S(2)}) copy-start(bf16[512,4,128]{2,0,1:T(8,128)(2,1)} %copy-done.5) | copy-start | bytes 1572868
  94.8 1.8 %copy-start.9 = (bf16[512,128]{1,0:T(8,128)(2,1)S(1)}, bf16[512,128]{1,0:T(8,128)(2,1)}, u32[]{:S(2)}) copy-start(bf16[512,128]{1,0:T(8,128)(2,1)} %fusion.29) | copy-start | bytes 393220
  99.7 2.9 %copy-start.4 = (pred[256,512]{0,1:T(8,128)(4,1)S(1)}, pred[256,512]{0,1:T(8,128)(4,1)}, u32[]{:S(2)}) copy-start(pred[256,512]{0,1:T(8,128)(4,1)} %iota_compare_fusion) | copy-start | bytes 393220
  102.6 2.1 %copy-start.2 = (bf16[256,4,128]{0,2,1:T(8,128)(2,1)S(1)}, bf16[256,4,128]{0,2,1:T(8,128)(2,1)}, u32[]{:S(2)}) copy-start(bf16[256,4,128]{0,2,1:T(8,128)(2,1)} %fusion.13) | copy-start | bytes 786436
Sparse Core Ops, SparseCore 0:
  9.5 52.5 all-gather.5
  63.6 21.4 all-gather.3
where the time goes:
time: 125 us; the launch traced here: 124 us
  waiting for transfers between devices  63.8 us (51%)
  between operations  13.7 us (11%)
  matrix products  13.5 us (11%)
  blocking collectives  11.2 us (9%)
  other arithmetic  9.01 us (7%)
  local copies, waits for them, and re-layouts  8.58 us (7%)
  starting transfers between devices  4.31 us (3%)
    all_gather x1, waiting for transfers between devices, body(): gathered = lax.all_gather(columns, 'dp', axis=0, tiled=True)  37.5 us
    all_gather x1, waiting for transfers between devices, body(): lax.all_gather(normed, 'sp', axis=0, tiled=True)  21.1 us
    all_to_all x1, blocking collectives, body(): lax.all_to_all(attended, 'sp', split_axis=0, concat_axis=1, tiled=True)  11.2 us
    all_to_all x1, waiting for transfers between devices, body(): lax.all_to_all(copied, 'sp', split_axis=2, concat_axis=0, tiled=True)  5.16 us
    unnamed x30, local copies, waits for them, and re-layouts  4.87 us
    dot_general x2, matrix products, body(): jnp.einsum('qhd,kd->hqk', mine[first:finish], key_heads[:finish], preferr...  4.85 us
    all_to_all x1, starting transfers between devices, body(): lax.all_to_all(copied, 'sp', split_axis=2, concat_axis=0, tiled=True)  4.26 us
    dot_general x1, matrix products, body(): jnp.dot(lax.all_gather(normed, 'sp', axis=0, tiled=True), gathered, prefe...  3.8 us
  transfers between devices with their start and end apart: 3, of which 3 were waited for; matrix products, arithmetic and copies ran while one was open for 7% of the time, Pallas kernels for 0%

commit v1 on v0

--- a/solution.py
+++ b/solution.py
@@ -56,7 +56,15 @@
     )
     gathered = lax.all_gather(columns, "dp", axis=0, tiled=True)
     queries = jnp.dot(
-        lax.all_gather(normed, "sp", axis=0, tiled=True),
+        jnp.concatenate(
+            lax.all_to_all(
+                jnp.stack([normed] * lax.axis_size("sp"), axis=0),
+                axis_name="sp",
+                split_axis=0,
+                concat_axis=0,
+            ),
+            axis=0,
+        ),
         gathered,
         preferred_element_type=jnp.float32,
     ).astype(jnp.bfloat16)

time: 125 us -> 104 us (0.83)
  waiting for transfers between devices: 63.8 us -> 35.8 us
  local copies, waits for them, and re-layouts: 8.58 us -> 16.3 us
  starting transfers between devices: 4.31 us -> 8.01 us
  other arithmetic: 9.01 us -> 5.43 us
    all_gather x1, waiting for transfers between devices: 37.5 us -> 6.4 us  [body(): gathered = lax.all_gather(columns, 'dp', axis=0, tiled=True)]
    all_to_all x0 -> x1, waiting for transfers between devices: none -> 24.1 us  [body(): lax.all_to_all(jnp.stack([normed] * lax.axis_size('sp'), axis=0), axis_na...]
    all_gather x1 -> x0, waiting for transfers between devices: 21.1 us -> none  [body(): lax.all_gather(normed, 'sp', axis=0, tiled=True)]
    all_to_all x0 -> x1, starting transfers between devices: none -> 3.74 us  [body(): lax.all_to_all(jnp.stack([normed] * lax.axis_size('sp'), axis=0), axis_na...]
    unnamed x30 -> x38, local copies, waits for them, and re-layouts: 4.87 us -> 8.27 us
    convert_element_type x3 -> x2, other arithmetic: 3.35 us -> 0.47 us  [rms_scaled(): return scaled.astype(jnp.bfloat16)]
    all_to_all x0 -> x1, local copies, waits for them, and re-layouts: none -> 2.72 us  [body(): lax.all_to_all(jnp.stack([normed] * lax.axis_size('sp'), axis=0), axis_na...]
    another operation x0 -> x1, local copies, waits for them, and re-layouts: none -> 1.63 us  [body(): jnp.stack([normed] * lax.axis_size('sp'), axis=0)]
  transfers between devices with their start and end apart: 3 -> 3, of which waited for: 3 -> 3; matrix products, arithmetic and copies ran while one was open for 7% -> 9% of each run, Pallas kernels for 0% -> 0%
where the time goes in v1:
time: 104 us; the launch traced here: 103 us
  waiting for transfers between devices  35.8 us (34%)
  local copies, waits for them, and re-layouts  16.3 us (16%)
  between operations  13.7 us (13%)
  matrix products  12.6 us (12%)
  blocking collectives  11.4 us (11%)
  starting transfers between devices  8.01 us (8%)
  other arithmetic  5.43 us (5%)
    all_to_all x1, waiting for transfers between devices, body(): lax.all_to_all(jnp.stack([normed] * lax.axis_size('sp'), axis=0), axis_na...  24.1 us
    all_to_all x1, blocking collectives, body(): lax.all_to_all(attended, 'sp', split_axis=0, concat_axis=1, tiled=True)  11.4 us
    unnamed x38, local copies, waits for them, and re-layouts  8.27 us
    all_gather x1, waiting for transfers between devices, body(): gathered = lax.all_gather(columns, 'dp', axis=0, tiled=True)  6.4 us
    all_to_all x1, waiting for transfers between devices, body(): lax.all_to_all(copied, 'sp', split_axis=2, concat_axis=0, tiled=True)  5.36 us
    all_to_all x1, starting transfers between devices, body(): lax.all_to_all(copied, 'sp', split_axis=2, concat_axis=0, tiled=True)  4.26 us
    dot_general x2, matrix products, body(): jnp.einsum('qhd,kd->hqk', mine[first:finish], key_heads[:finish], preferr...  4.02 us
    dot_general x1, matrix products, body(): jnp.dot(jnp.concatenate(lax.all_to_all(jnp.stack([normed] * lax.axis_size...  3.77 us
  transfers between devices with their start and end apart: 3, of which 3 were waited for; matrix products, arithmetic and copies ran while one was open for 9% of the time, Pallas kernels for 0%

profile of v1, /device:TPU:0, one launch (start us, length us, event | category | flops | bytes accessed | tf_op | source)
XLA Modules:
  0.0 103.3 jit_solution(6314977315177437642)
XLA Ops:
  6.6 1.2 %copy-done = bf16[258,2048]{1,0:T(8,128)(2,1)S(1)} copy-done((bf16[258,2048]{1,0:T(8,128)(2,1)S(1)}, bf16[258,2048]{1,0:T(8,128)(2,1)}, u32[]{:S(2)}) %copy-start) | copy-done | bytes 1056792
  8.5 1.0 copy.57
  9.6 1.0 copy.58
  10.6 0.8 copy.59
  11.5 4.3 %all-to-all-start = ((bf16[128,2,4,128]{3,0,1,2:T(8,128)(2,1)}), bf16[128,2,4,128]{3,0,1,2:T(8,128)(2,1)S(1)}, u32[]{:S(2)}, u32[]{:S(2)}) async-start(bf16[128,2,4,128]{3,0,1,2:T(8,128)(2,1)} %copy.59), calls=%async_computation | async-start | bytes 524288 | tf_op jit(solution)/shard_map/all_to_all | solution.py:51
  16.4 5.4 %all-to-all-done = bf16[128,2,4,128]{3,0,1,2:T(8,128)(2,1)S(1)} async-done(((bf16[128,2,4,128]{3,0,1,2:T(8,128)(2,1)}), bf16[128,2,4,128]{3,0,1,2:T(8,128)(2,1)S(1)}, u32[]{:S(2)}, u32[]{:S(2)}) %all-to-all-start) | async-done | bytes 262176 | tf_op jit(solution)/shard_map/all_to_all | solution.py:51
  21.7 1.6 %stack.20 = bf16[4,128,2064]{1,2,0:T(8,128)(2,1)} broadcast(bf16[128,2064]{0,1:T(8,128)(2,1)S(1)} %fusion.27), dimensions={1,2} | broadcast | bytes 2641920 | tf_op jit(solution)/shard_map/stack | solution.py:61
  23.4 3.7 %all-to-all-start.1 = ((bf16[4,128,2064]{1,2,0:T(8,128)(2,1)}), bf16[4,128,2064]{1,2,0:T(8,128)(2,1)S(1)}, u32[]{:S(2)}, u32[]{:S(2)}) async-start(bf16[4,128,2064]{1,2,0:T(8,128)(2,1)} %stack.20), calls=%async_computation.1 | async-start | bytes 4227072 | tf_op jit(solution)/shard_map/all_to_all | solution.py:60
  27.3 0.7 iota_compare_fusion
  28.9 24.1 %all-to-all-done.1 = bf16[4,128,2064]{1,2,0:T(8,128)(2,1)S(1)} async-done(((bf16[4,128,2064]{1,2,0:T(8,128)(2,1)}), bf16[4,128,2064]{1,2,0:T(8,128)(2,1)S(1)}, u32[]{:S(2)}, u32[]{:S(2)}) %all-to-all-start.1) | async-done | bytes 2113568 | tf_op jit(solution)/shard_map/all_to_all | solution.py:60
  52.9 2.7 %copy.61 = bf16[4,128,2064]{2,1,0:T(8,128)(2,1)} copy(bf16[4,128,2064]{1,2,0:T(8,128)(2,1)S(1)} %all-to-all-done.1) | data formatting | bytes 4227072 | tf_op jit(solution)/shard_map/all_to_all | solution.py:60
  55.7 6.4 %all-gather.3.cloned.1.call-done = bf16[8,258,512]{2,1,0:T(8,128)(2,1)} async-done(((bf16[1,258,512]{2,1,0:T(8,128)(2,1)}), bf16[8,258,512]{2,1,0:T(8,128)(2,1)}) %all-gather.3.cloned.1.call-update) | async-done | bytes 2113552 | tf_op jit(solution)/shard_map/all_gather | solution.py:57
  62.1 2.9 %reshape.107 = bf16[2064,512]{1,0:T(8,128)(2,1)} reshape(bf16[8,258,512]{2,1,0:T(8,128)(2,1)} %all-gather.3.cloned.1.call-done) | data formatting | bytes 4227072
  65.0 3.8 %convolution_convert_fusion = bf16[512,512]{1,0:T(8,128)(2,1)} fusion(bf16[512,2064]{1,0:T(8,128)(2,1)S(1)} %bitcast.98, bf16[2064,512]{1,0:T(8,128)(2,1)} %reshape.107), kind=kOutput, calls=%fused_computation.26 | convolution fusion | flops 1082392576 | bytes 4751360 | tf_op jit(solution)/shard_map/dot_general | solution.py:58
  68.7 1.4 %reshape.105 = f32[512,4,128]{2,1,0:T(4,128)S(1)} reshape(bf16[512,512]{1,0:T(8,128)(2,1)} %convolution_convert_fusion) | data formatting | bytes 1572864 | tf_op jit(solution)/shard_map/convert_element_type | solution.py:13
  71.3 0.8 copy-done.9
  72.1 0.9 bitcast_reduce_fusion.1
  73.8 0.8 fusion.22
  74.6 1.0 fusion.13
  75.6 3.1 %bitcast_reduce_fusion = (f32[4,256,4]{1,2,0:T(4,128)S(1)}, f32[4,256,512]{1,2,0:T(8,128)}, f32[512,256,4]{1,0,2:T(8,128)S(1)}) fusion(f32[4]{0:T(128)S(1)} %dynamic_slice.7, pred[256,512]{0,1:T(8,128)(4,1)S(1)} %copy-done.7, bf16[512,4,128]{2,0,1:T(8,128)(2,1)S(1)} %copy-done.10, bf16[512,128]{1,0:T(8,128)(2,1)S(1)} %copy-done.12), kind=kOutput, calls=%fused_computation.71 | convolution fusion | flops 139980800 | bytes 4735488 | tf_op jit(solution)/shard_map/qhd,kd->hqk/dot_general | solution.py:81
  78.7 2.9 %convolution_add_fusion = f32[4,256,4,128]{1,3,2,0:T(8,128)S(1)} fusion(f32[4,256,4,128]{1,3,2,0:T(8,128)} %bitcast.99, f32[4,256,4]{1,2,0:T(4,128)S(1)} %sub.15), kind=kOutput, calls=%fused_computation.19 | convolution fusion | flops 805847040 | bytes 4210688 | tf_op jit(solution)/shard_map/hqbk,kj->hqbj/dot_general | solution.py:31
  81.6 1.8 %fusion.4 = bf16[4,256,512]{1,2,0:T(8,128)(2,1)S(1)} fusion(f32[4,256,4,128]{1,3,2,0:T(8,128)S(1)} %convolution_add_fusion, f32[512,256,4]{1,0,2:T(8,128)S(1)} %get-tuple-element.9, f32[4]{0:T(128)S(1)} %dynamic_slice.7, pred[256,512]{0,1:T(8,128)(4,1)S(1)} %copy-done.8), kind=kLoop, calls=%fused_computation.8 | loop fusion | flops 6815744 | bytes 5373968 | tf_op jit(solution)/shard_map/convert_element_type | solution.py:88
  84.0 11.4 %all_to_all.33 = bf16[4,128,512]{1,2,0:T(8,128)(2,1)S(1)} all-to-all(bf16[4,128,512]{1,2,0:T(8,128)(2,1)S(1)} %copy.70), channel_id=1, replica_groups=mesh['sp'=4,'dp'=8] {'sp'}, dimensions={0} | all-to-all | bytes 1048576 | tf_op jit(solution)/shard_map/all_to_all | solution.py:99
  95.4 1.0 copy.71
  (59 shorter events, 4.8 us)
Async XLA Ops:
  6.5 1.2 %copy-start = (bf16[258,2048]{1,0:T(8,128)(2,1)S(1)}, bf16[258,2048]{1,0:T(8,128)(2,1)}, u32[]{:S(2)}) copy-start(bf16[258,2048]{1,0:T(8,128)(2,1)} %param.10) | copy-start | bytes 3170308
  6.5 9.2 %copy-start.2 = (bf16[1,128,2064]{1,2,0:T(8,128)(2,1)S(1)}, bf16[1,128,2064]{1,2,0:T(8,128)(2,1)}, u32[]{:S(2)}) copy-start(bf16[1,128,2064]{1,2,0:T(8,128)(2,1)} %param.8) | copy-start | bytes 1585156
  6.5 9.5 %copy-start.13 = (f32[2064]{0:T(1024)S(1)}, f32[2064]{0:T(1024)}, u32[]{:S(2)}) copy-start(f32[2064]{0:T(1024)} %param.9) | copy-start | bytes 24772
  6.5 55.5 %all-gather.3.cloned.1.call-start = ((), (), s32[]{:S(2)}) async-start(), calls=%async_computation.3 | async-start | bytes 2433024 | tf_op jit(solution)/shard_map/all_gather | solution.py:57
  11.5 10.3 %all-to-all-start = ((bf16[128,2,4,128]{3,0,1,2:T(8,128)(2,1)}), bf16[128,2,4,128]{3,0,1,2:T(8,128)(2,1)S(1)}, u32[]{:S(2)}, u32[]{:S(2)}) async-start(bf16[128,2,4,128]{3,0,1,2:T(8,128)(2,1)} %copy.59), calls=%async_computation | async-start | bytes 524288 | tf_op jit(solution)/shard_map/all_to_all | solution.py:51
  23.4 3.8 %copy-start.16 = (f32[16]{0:T(128)S(1)}, f32[16]{0:T(128)}, u32[]{:S(2)}) copy-start(f32[16]{0:T(128)} %param.15) | copy-start | bytes 196
  23.4 5.4 %copy-start.14 = (f32[128]{0:T(128)S(1)}, f32[128]{0:T(128)}, u32[]{:S(2)}) copy-start(f32[128]{0:T(128)} %param.13) | copy-start | bytes 1540
  23.4 29.6 %all-to-all-start.1 = ((bf16[4,128,2064]{1,2,0:T(8,128)(2,1)}), bf16[4,128,2064]{1,2,0:T(8,128)(2,1)S(1)}, u32[]{:S(2)}, u32[]{:S(2)}) async-start(bf16[4,128,2064]{1,2,0:T(8,128)(2,1)} %stack.20), calls=%async_computation.1 | async-start | bytes 4227072 | tf_op jit(solution)/shard_map/all_to_all | solution.py:60
  28.0 0.7 copy-start.4
  28.9 42.4 %copy-start.11 = (bf16[512,128]{1,0:T(8,128)(2,1)}, bf16[512,128]{1,0:T(8,128)(2,1)S(1)}, u32[]{:S(2)}) copy-start(bf16[512,128]{1,0:T(8,128)(2,1)S(1)} %fusion.30) | copy-start | bytes 393220
  55.7 9.3 %copy-start.1 = (bf16[4,128,2064]{2,1,0:T(8,128)(2,1)S(1)}, bf16[4,128,2064]{2,1,0:T(8,128)(2,1)}, u32[]{:S(2)}) copy-start(bf16[4,128,2064]{2,1,0:T(8,128)(2,1)} %copy.61) | copy-start | bytes 6340612
  68.7 2.2 %copy-start.3 = (bf16[512,512]{1,0:T(8,128)(2,1)S(1)}, bf16[512,512]{1,0:T(8,128)(2,1)}, u32[]{:S(2)}) copy-start(bf16[512,512]{1,0:T(8,128)(2,1)} %convolution_convert_fusion) | copy-start | bytes 1572868
  68.7 2.2 %copy-start.15 = (f32[128]{0:T(128)S(1)}, f32[128]{0:T(128)}, u32[]{:S(2)}) copy-start(f32[128]{0:T(128)} %param.11) | copy-start | bytes 1540
  71.3 0.8 copy-start.9
  73.1 1.5 %copy-start.5 = (bf16[4,128,2,1,128]{4,1,0,2,3:T(8,128)(2,1)S(1)}, bf16[4,128,2,1,128]{4,1,0,2,3:T(8,128)(2,1)}, u32[]{:S(2)}) copy-start(bf16[4,128,2,1,128]{4,1,0,2,3:T(8,128)(2,1)} %copy-done.4) | copy-start | bytes 786436
  73.8 1.8 %copy-start.7 = (pred[256,512]{0,1:T(8,128)(4,1)S(1)}, pred[256,512]{0,1:T(8,128)(4,1)}, u32[]{:S(2)}) copy-start(pred[256,512]{0,1:T(8,128)(4,1)} %iota_compare_fusion) | copy-start | bytes 393220
  73.8 1.8 %copy-start.10 = (bf16[512,4,128]{2,0,1:T(8,128)(2,1)S(1)}, bf16[512,4,128]{2,0,1:T(8,128)(2,1)}, u32[]{:S(2)}) copy-start(bf16[512,4,128]{2,0,1:T(8,128)(2,1)} %copy-done.9) | copy-start | bytes 1572868
  73.8 1.8 %copy-start.12 = (bf16[512,128]{1,0:T(8,128)(2,1)S(1)}, bf16[512,128]{1,0:T(8,128)(2,1)}, u32[]{:S(2)}) copy-start(bf16[512,128]{1,0:T(8,128)(2,1)} %copy-done.11) | copy-start | bytes 393220
  78.7 2.9 %copy-start.8 = (pred[256,512]{0,1:T(8,128)(4,1)S(1)}, pred[256,512]{0,1:T(8,128)(4,1)}, u32[]{:S(2)}) copy-start(pred[256,512]{0,1:T(8,128)(4,1)} %iota_compare_fusion) | copy-start | bytes 393220
  81.6 2.2 %copy-start.6 = (bf16[256,4,128]{0,2,1:T(8,128)(2,1)S(1)}, bf16[256,4,128]{0,2,1:T(8,128)(2,1)}, u32[]{:S(2)}) copy-start(bf16[256,4,128]{0,2,1:T(8,128)(2,1)} %fusion.13) | copy-start | bytes 786436
Sparse Core Ops, SparseCore 0:
  9.5 52.5 all-gather.2
